TPU v7x, 256 devices: a whole 4x4x8 slice. The times are simulated.
256 devices in a mesh: sp: 64 (over z, x, core), tp: 4 (over y).
Axes of the slice: x: 4, y: 4, z: 8, core: 2. Of those that a mesh axis runs over, the one named last changes fastest.
Arguments:
- hidden_in: bfloat16 [16384, 2048], P('sp'), may hold values from -6 to 6
- cotangent: bfloat16 [16384, 2048], P('sp'), may hold values from -16 to 16
- routes: int32 [16384, 2], P('sp'), may hold values from 0 to 63, all different within a row; in each aligned block of 256 rows (0 to 255, 256 to 511, ...) at most 12 rows name the same one
- routing_weights: float32 [16384, 2], P('sp'), may hold values from 0.1 to 1
- w_gate: bfloat16 [64, 2048, 1024], P('sp', None, 'tp'), may hold values from -0.125 to 0.125
- w_up: bfloat16 [64, 2048, 1024], P('sp', None, 'tp'), may hold values from -0.125 to 0.125
- w_down: bfloat16 [64, 1024, 2048], P('sp', 'tp'), may hold values from -0.1875 to 0.1875
- b_gate: bfloat16 [16384, 1024], P('sp', 'tp'), may hold values from -6 to 6
- c_gate: bfloat16 [16384, 1024], P('sp', 'tp'), may hold values from -6 to 6
- x_in: bfloat16 [16384, 1024], P('sp', 'tp'), may hold values from -6 to 6
- taps: bfloat16 [3, 1024], P(None, 'tp'), may hold values from -3 to 3
- w_out: bfloat16 [2048, 1024], P(None, 'tp'), may hold values from -0.1875 to 0.1875
Outputs:
- grad_gate: bfloat16 [64, 2048, 1024], P('sp', None, 'tp')
- grad_up: bfloat16 [64, 2048, 1024], P('sp', None, 'tp')
- grad_down: bfloat16 [64, 1024, 2048], P('sp', 'tp')
- out_proj_grad: float32 [2048, 1024], P('sp', 'tp')
- residual_grad: bfloat16 [16384, 2048], P('sp', 'tp')
- grad_b: bfloat16 [16384, 1024], P('sp', 'tp')
- grad_c: bfloat16 [16384, 1024], P('sp', 'tp')
- grad_x: bfloat16 [16384, 1024], P('sp', 'tp')
Inputs may be any that keep to these rules, and one draw needn't show every extreme that they name: `routes`: each row names 2 different experts. Among the rows of one index of sp no expert is named more than 12 times, a bound that some block reaches in some of them.
All inputs are finite; a program needn't handle non-finite values.
Results may differ from a plain program's by a relative error of at most 0.01.
Values may be sent and summed in bfloat16 or wider, within the bound.
No kernel may reach another device: no remote copies, remote signals or barrier semaphores. Data moves between devices by JAX's collectives and lax.ppermute only.
A program may use at most 64 MiB of HBM per device.

v0:
```python
import jax
import jax.numpy as jnp
from jax import lax
from jax.sharding import PartitionSpec as P


def in_one_piece(arrays, axis, split_dim, concat_dim, along):
    widths = [a.shape[along] for a in arrays]
    both = jnp.concatenate(arrays, axis=along)
    whole = lax.all_to_all(both, axis, split_axis=split_dim, concat_axis=concat_dim, tiled=True)
    return tuple(jnp.split(whole, [sum(widths[:k]) for k in range(1, len(widths))], axis=along))


def sent_together(arrays, axis, dim, along):
    ends, at = ([], 0)
    for a in arrays[:-1]:
        at += a.shape[along]
        ends.append(at)
    both = jnp.concatenate(arrays, axis=along)
    return tuple(jnp.split(lax.all_gather(both, axis, axis=dim, tiled=True), ends, axis=along))


def cut_along(x, dim, devices):
    before, after = (x.shape[:dim], x.shape[dim + 1 :])
    return jnp.moveaxis(x.reshape(*before, devices, -1, *after), dim, 0)


def summed_on_arrival(x, axis, dim):
    blocks = cut_along(x, dim, lax.axis_size(axis))
    arrived = lax.all_to_all(blocks, axis, split_axis=0, concat_axis=0, tiled=True)
    return arrived.astype(jnp.float32).sum(axis=0)


def laid_out(blocks, dim):
    lengths = list(blocks.shape[1:])
    lengths[dim] *= blocks.shape[0]
    return jnp.moveaxis(blocks, 0, dim).reshape(lengths)


def copy_for_each(x, axis):
    copies = jnp.broadcast_to(x, (lax.axis_size(axis), *x.shape))
    return lax.all_to_all(copies, axis, split_axis=0, concat_axis=0, tiled=True)


def gathered_copies(x, axis, dim):
    return laid_out(copy_for_each(x, axis), dim)


def from_behind(x, axis, by):
    devices = lax.axis_size(axis)
    pairs = [(i, i + by) for i in range(devices) if 0 <= i + by < devices]
    return lax.ppermute(x, axis, pairs)


def per_device(
    hidden_in,
    cotangent,
    routes,
    routing_weights,
    w_gate,
    w_up,
    w_down,
    b_gate,
    c_gate,
    x_in,
    taps,
    w_out,
):
    tok_rows, model_width = hidden_in.shape
    top_k = routes.shape[1]
    local_experts = w_gate.shape[0]
    sp_size = lax.axis_size("sp")
    tp_size = lax.axis_size("tp")
    experts = local_experts * sp_size
    capacity = 3 * tok_rows * top_k // (2 * experts)
    slot_count = tok_rows * top_k
    feature_share = model_width // tp_size
    share_offset = lax.axis_index("tp") * feature_share
    flat_ids = routes.reshape(-1)
    onehot = (flat_ids[:, None] == jnp.arange(experts, dtype=jnp.int32)[None, :]).astype(jnp.int32)
    before = jnp.cumsum(onehot, axis=0) - onehot
    position = jnp.sum(before * onehot, axis=1)
    target = flat_ids * capacity + position
    source = (
        jnp.full((experts * capacity,), slot_count, jnp.int32)
        .at[target]
        .set(jnp.arange(slot_count, dtype=jnp.int32))
    )
    filled = source < slot_count
    clipped = jnp.minimum(source, slot_count - 1)
    token_of = clipped // top_k
    weight_of = jnp.where(filled, routing_weights.reshape(-1)[clipped], 0.0)
    rows_src = lax.dynamic_slice_in_dim(hidden_in, share_offset, feature_share, 1)
    cot_src = lax.dynamic_slice_in_dim(cotangent, share_offset, feature_share, 1)
    send_rows = jnp.where(filled[:, None], rows_src[token_of], jnp.zeros((), jnp.bfloat16))
    send_rows = send_rows.reshape(experts, capacity, -1)
    send_cot = (weight_of[:, None] * cot_src[token_of].astype(jnp.float32)).astype(jnp.bfloat16)
    send_cot = send_cot.reshape(experts, capacity, -1)
    part_rows, part_cot = in_one_piece((send_rows, send_cot), "sp", 0, 1, 2)
    rows_h, rows_s = sent_together((part_rows, part_cot), "tp", 2, 0)
    pre_gate = jnp.einsum("erd,edf->erf", rows_h, w_gate, preferred_element_type=jnp.float32)
    pre_up = jnp.einsum("erd,edf->erf", rows_h, w_up, preferred_element_type=jnp.float32)
    sigma = jax.nn.sigmoid(pre_gate)
    silu_gate = pre_gate * sigma
    hid = (silu_gate * pre_up).astype(jnp.bfloat16)
    d_hid = jnp.einsum("erd,efd->erf", rows_s, w_down, preferred_element_type=jnp.float32)
    d_up = (d_hid * silu_gate).astype(jnp.bfloat16)
    d_pre = (d_hid * pre_up * sigma * (1.0 + pre_gate * (1.0 - sigma))).astype(jnp.bfloat16)
    grad_down = jnp.einsum("erf,erd->efd", hid, rows_s, preferred_element_type=jnp.float32).astype(
        jnp.bfloat16
    )
    grad_gate = jnp.einsum(
        "erd,erf->edf", rows_h, d_pre, preferred_element_type=jnp.float32
    ).astype(jnp.bfloat16)
    grad_up = jnp.einsum("erd,erf->edf", rows_h, d_up, preferred_element_type=jnp.float32).astype(
        jnp.bfloat16
    )
    partial_grad = jnp.einsum("erf,edf->erd", d_pre, w_gate, preferred_element_type=jnp.float32)
    partial_grad = partial_grad + jnp.einsum(
        "erf,edf->erd", d_up, w_up, preferred_element_type=jnp.float32
    )
    partial_low = partial_grad.astype(jnp.bfloat16)
    shared_rows = summed_on_arrival(partial_low, "tp", 2).astype(jnp.bfloat16)
    back = lax.all_to_all(shared_rows, "sp", split_axis=1, concat_axis=0, tiled=True)
    back_flat = back.reshape(experts * capacity, feature_share)
    per_token = back_flat[target].astype(jnp.float32).reshape(tok_rows, top_k, feature_share)
    own_cot = lax.dynamic_slice_in_dim(cotangent, share_offset, feature_share, 1).astype(
        jnp.float32
    )
    residual_grad = (own_cot + jnp.sum(per_token, axis=1)).astype(jnp.bfloat16)
    full_grad = gathered_copies(residual_grad, "tp", 1)
    taps_f = taps.astype(jnp.float32)
    gated = c_gate.astype(jnp.float32) * x_in.astype(jnp.float32)
    earlier = from_behind(gated[tok_rows - 2 :], "sp", 1)
    padded = jnp.concatenate([earlier, gated], axis=0)
    conv = (
        taps_f[0] * padded[0:tok_rows]
        + taps_f[1] * padded[1 : tok_rows + 1]
        + taps_f[2] * padded[2 : tok_rows + 2]
    )
    b_f = b_gate.astype(jnp.float32)
    y_short = (b_f * conv).astype(jnp.bfloat16)
    d_y = jnp.dot(full_grad, w_out, preferred_element_type=jnp.float32)
    grad_b = (d_y * conv).astype(jnp.bfloat16)
    d_conv = b_f * d_y
    following = from_behind(d_conv[0:2], "sp", -1)
    later = jnp.concatenate([d_conv, following], axis=0)
    d_v = (
        taps_f[2] * later[0:tok_rows]
        + taps_f[1] * later[1 : tok_rows + 1]
        + taps_f[0] * later[2 : tok_rows + 2]
    )
    grad_c = (d_v * x_in.astype(jnp.float32)).astype(jnp.bfloat16)
    grad_x = (d_v * c_gate.astype(jnp.float32)).astype(jnp.bfloat16)
    out_proj_grad = summed_on_arrival(
        jnp.einsum("td,tc->dc", full_grad, y_short, preferred_element_type=jnp.float32).astype(
            jnp.bfloat16
        ),
        "sp",
        0,
    )
    return (grad_gate, grad_up, grad_down, out_proj_grad, residual_grad, grad_b, grad_c, grad_x)


def solution(mesh):
    return jax.shard_map(
        per_device,
        mesh=mesh,
        in_specs=(
            P("sp", None),
            P("sp", None),
            P("sp", None),
            P("sp", None),
            P("sp", None, "tp"),
            P("sp", None, "tp"),
            P("sp", "tp", None),
            P("sp", "tp"),
            P("sp", "tp"),
            P("sp", "tp"),
            P(None, "tp"),
            P(None, "tp"),
        ),
        out_specs=(
            P("sp", None, "tp"),
            P("sp", None, "tp"),
            P("sp", "tp", None),
            P("sp", "tp"),
            P("sp", "tp"),
            P("sp", "tp"),
            P("sp", "tp"),
            P("sp", "tp"),
        ),
        check_vma=False,
    )
```

profile of v0, /device:TPU:1, one launch (start us, length us, event | category | flops | bytes accessed | tf_op | source)
XLA Modules:
  0.0 338.7 jit_solution(15847824969472595862)
XLA Ops:
  7.2 0.8 broadcast_multiply_fusion
  8.0 0.8 copy.34
  8.8 0.1 eq.25
  9.0 0.1 eq.29
  9.2 0.1 mul.129
  9.4 1.2 reduce-window.6
  10.6 0.2 slice_reduce_fusion
  11.0 2.4 scatter_custom_fusion
  13.5 1.0 constant_dynamic-slice_fusion
  14.5 3.3 gather_fusion.2
  17.8 1.2 reshape.179
  19.2 0.1 reshape.169
  19.4 5.0 %gather_fusion.1 = f32[768]{0:T(1024)S(1)} fusion(f32[512]{0:T(512)S(1)} %reshape.169, s32[1024]{0:T(1024)S(1)} %get-tuple-element.24), kind=kCustom, calls=%fused_computation.1 | custom fusion | bytes 9216 | tf_op jit(solution)/shard_map/gather | solution.py:92
  24.5 1.0 constant_dynamic-slice_fusion.1
  25.5 3.3 gather_fusion
  28.8 2.1 gather.15
  31.0 0.2 multiply_convert_fusion
  31.2 1.0 copy-done.2
  32.2 0.2 broadcast_select_fusion
  32.4 0.3 pad_maximum_fusion
  32.8 62.5 %all_to_all.36 = bf16[64,12,1024]{2,1,0:T(8,128)(2,1)S(1)} all-to-all(bf16[64,12,1024]{2,1,0:T(8,128)(2,1)S(1)} %pad_maximum_fusion), channel_id=1, replica_groups=mesh['sp'=64,'tp'=4] {'sp'}, dimensions={0} | all-to-all | bytes 3145728 | tf_op jit(solution)/shard_map/all_to_all | solution.py:10
  95.2 1.3 all_to_all.26
  96.6 1.5 fusion.41
  98.1 1.3 pad_maximum_fusion.1
  99.4 66.0 %all-gather.2.cloned.1.call-done = bf16[2,768,2048]{2,1,0:T(8,128)(2,1)} async-done(((bf16[2,768,512]{2,1,0:T(8,128)(2,1)}), bf16[2,768,2048]{2,1,0:T(8,128)(2,1)}) %all-gather.2.cloned.1.call-update) | async-done | bytes 6291472 | tf_op jit(solution)/shard_map/all_gather | solution.py:20
  165.3 3.0 fusion.6
  168.4 0.7 copy-done.14
  169.1 1.0 fusion.7
  170.1 0.5 copy-done.15
  170.6 1.2 multiply_convert_fusion.2
  171.8 1.0 fusion.8
  172.8 2.8 add_convert_fusion
  175.6 4.8 %reshape.175 = bf16[1,768,4,512]{3,2,1,0:T(4,128)(2,1)S(1)} reshape(bf16[768,2048]{1,0:T(8,128)(2,1)} %add_convert_fusion) | data formatting | bytes 6291456 | tf_op jit(solution)/shard_map/reshape | solution.py:25
  180.4 0.6 copy.47
  181.1 39.7 %all_to_all.37 = bf16[4,1,768,512]{3,2,1,0:T(8,128)(2,1)S(1)} all-to-all(bf16[4,1,768,512]{3,2,1,0:T(8,128)(2,1)S(1)} %bitcast.84), channel_id=1, replica_groups=mesh['sp'=64,'tp'=4] {'tp'}, dimensions={0} | all-to-all | bytes 6291456 | tf_op jit(solution)/shard_map/all_to_all | solution.py:30
  220.8 1.6 reduce_sum.45
  222.4 2.3 copy.49
  224.7 0.5 broadcast.112
  225.2 5.4 %reduce.4 = bf16[768,512]{1,0:T(8,128)(2,1)S(1)} reduce(bf16[768,1,512]{2,1,0:T(2,128)(2,1)S(1)} %bitcast.87, bf16[]{:T(256)} %broadcast.112), dimensions={1}, to_apply=%bitcast.82.reduce_sub_computation | reduce | bytes 1572866
  230.7 1.2 reshape.227
  231.9 12.0 %all-to-all-start.2 = ((bf16[64,2,3072]{2,1,0:T(2,128)(2,1)}), bf16[64,2,3072]{2,1,0:T(2,128)(2,1)S(1)}, u32[]{:S(2)}, u32[]{:S(2)}) async-start(bf16[64,2,3072]{2,1,0:T(2,128)(2,1)} %reshape.227), calls=%async_computation.2 | async-start | bytes 1572864 | tf_op jit(solution)/shard_map/all_to_all | solution.py:124
  243.9 23.0 %all-to-all-done.2 = bf16[64,2,3072]{2,1,0:T(2,128)(2,1)S(1)} async-done(((bf16[64,2,3072]{2,1,0:T(2,128)(2,1)}), bf16[64,2,3072]{2,1,0:T(2,128)(2,1)S(1)}, u32[]{:S(2)}, u32[]{:S(2)}) %all-to-all-start.2) | async-done | bytes 786464 | tf_op jit(solution)/shard_map/all_to_all | solution.py:124
  266.9 0.6 reshape.228
  267.5 0.2 copy.48
  267.7 2.0 gather_fusion.3
  269.7 0.7 reshape.180
  270.4 1.2 reduce_sum.47
  271.6 1.0 add_convert_fusion.1
  272.8 1.0 broadcast_in_dim.39
  273.9 3.8 %all-to-all-start.3 = ((bf16[4,256,512]{1,2,0:T(8,128)(2,1)}), bf16[4,256,512]{1,2,0:T(8,128)(2,1)S(1)}, u32[]{:S(2)}, u32[]{:S(2)}) async-start(bf16[4,256,512]{1,2,0:T(8,128)(2,1)} %broadcast_in_dim.39), calls=%async_computation.3 | async-start | bytes 2097152 | tf_op jit(solution)/shard_map/all_to_all | solution.py:42
  277.7 3.7 %collective-permute-start = (f32[2,256]{1,0:T(2,128)S(1)}, f32[2,256]{1,0:T(2,128)S(1)}, u32[]{:S(2)}, u32[]{:S(2)}) collective-permute-start(f32[2,256]{1,0:T(2,128)S(1)} %slice.57), channel_id=1, source_target_pairs={{0,4},{4,8},{8,12},{12,16},{16,20},{20,24},{24,28},{28,32},{32,36}... | collective-permute-start | bytes 6152 | tf_op jit(solution)/shard_map/ppermute | solution.py:52
  281.4 0.7 collective-permute-done
  282.1 9.7 %all-to-all-done.3 = bf16[4,256,512]{1,2,0:T(8,128)(2,1)S(1)} async-done(((bf16[4,256,512]{1,2,0:T(8,128)(2,1)}), bf16[4,256,512]{1,2,0:T(8,128)(2,1)S(1)}, u32[]{:S(2)}, u32[]{:S(2)}) %all-to-all-start.3) | async-done | bytes 1048608 | tf_op jit(solution)/shard_map/all_to_all | solution.py:42
  291.9 2.0 multiply_convert_fusion.5
  293.9 2.3 convolution_convert_fusion
  296.2 6.6 %all-to-all-start.4 = ((bf16[64,32,256]{2,1,0:T(8,128)(2,1)}), bf16[64,32,256]{2,1,0:T(8,128)(2,1)S(1)}, u32[]{:S(2)}, u32[]{:S(2)}) async-start(bf16[64,32,256]{2,1,0:T(8,128)(2,1)} %bitcast.18), calls=%async_computation.4 | async-start | bytes 2097152 | tf_op jit(solution)/shard_map/all_to_all | solution.py:30
  302.9 4.0 %fusion.3 = bf16[1,2048,256]{2,1,0:T(8,128)(2,1)} fusion(bf16[768,256]{1,0:T(8,128)(2,1)S(1)} %get-tuple-element.15, bf16[2,768,2048]{2,1,0:T(8,128)(2,1)} %all-gather.2.cloned.1.call-done), kind=kOutput, calls=%fused_computation.15 | convolution fusion | flops 805830656 | bytes 4587520 | tf_op jit(solution)/shard_map/erd,erf->edf/dot_general | solution.py:112
  306.9 4.0 %fusion.5 = bf16[1,256,2048]{2,1,0:T(8,128)(2,1)} fusion(bf16[2,768,2048]{2,1,0:T(8,128)(2,1)} %all-gather.2.cloned.1.call-done, f32[768,256]{1,0:T(8,128)S(1)} %copy-done.19, f32[768,256]{1,0:T(8,128)S(1)} %copy-done.17), kind=kOutput, calls=%fused_computation.17 | convolution fusion | flops 807010304 | bytes 5767168 | tf_op jit(solution)/shard_map/erf,erd->efd/dot_general | solution.py:109
  310.9 2.5 collective-permute-start.1
  313.4 4.0 %fusion.4 = bf16[1,2048,256]{2,1,0:T(8,128)(2,1)} fusion(bf16[768,256]{1,0:T(8,128)(2,1)S(1)} %copy-done.11, bf16[2,768,2048]{2,1,0:T(8,128)(2,1)} %all-gather.2.cloned.1.call-done), kind=kOutput, calls=%fused_computation.16 | convolution fusion | flops 805830656 | bytes 4587520 | tf_op jit(solution)/shard_map/erd,erf->edf/dot_general | solution.py:115
  317.4 0.8 fusion.24
  318.2 0.7 fusion.25
  318.9 12.2 %all-to-all-done.4 = bf16[64,32,256]{2,1,0:T(8,128)(2,1)S(1)} async-done(((bf16[64,32,256]{2,1,0:T(8,128)(2,1)}), bf16[64,32,256]{2,1,0:T(8,128)(2,1)S(1)}, u32[]{:S(2)}, u32[]{:S(2)}) %all-to-all-start.4) | async-done | bytes 1048608 | tf_op jit(solution)/shard_map/all_to_all | solution.py:30
  331.0 0.8 convert_reduce_fusion
  (59 shorter events, 1.0 us)
Async XLA Ops:
  7.2 158.2 %copy-start = (bf16[1,2048,256]{2,1,0:T(8,128)(2,1)S(1)}, bf16[1,2048,256]{2,1,0:T(8,128)(2,1)}, u32[]{:S(2)}) copy-start(bf16[1,2048,256]{2,1,0:T(8,128)(2,1)} %param.16) | copy-start | bytes 3145732
  7.2 158.2 %all-gather.2.cloned.1.call-start = ((), (), s32[]{:S(2)}) async-start(), calls=%async_computation.5 | async-start | bytes 7864320 | tf_op jit(solution)/shard_map/all_gather | solution.py:20
  14.5 4.6 %copy-start.13 = (f32[256,2]{0,1:T(2,128)S(1)}, f32[256,2]{0,1:T(2,128)}, u32[]{:S(2)}) copy-start(f32[256,2]{0,1:T(2,128)} %param.15) | copy-start | bytes 6148
  31.0 1.2 copy-start.2
  99.4 69.0 %copy-start.5 = (bf16[1,2048,256]{2,1,0:T(8,128)(2,1)S(1)}, bf16[1,2048,256]{2,1,0:T(8,128)(2,1)}, u32[]{:S(2)}) copy-start(bf16[1,2048,256]{2,1,0:T(8,128)(2,1)} %param.17) | copy-start | bytes 3145732
  165.3 3.7 %copy-start.14 = (bf16[2,768,2048]{2,1,0:T(8,128)(2,1)S(1)}, bf16[2,768,2048]{2,1,0:T(8,128)(2,1)}, u32[]{:S(2)}) copy-start(bf16[2,768,2048]{2,1,0:T(8,128)(2,1)} %all-gather.2.cloned.1.call-done) | copy-start | bytes 18874372
  169.1 1.0 copy-start.16
  169.1 1.5 copy-start.15
  170.6 1.2 copy-start.18
  171.8 1.0 copy-start.10
  231.9 35.0 %all-to-all-start.2 = ((bf16[64,2,3072]{2,1,0:T(2,128)(2,1)}), bf16[64,2,3072]{2,1,0:T(2,128)(2,1)S(1)}, u32[]{:S(2)}, u32[]{:S(2)}) async-start(bf16[64,2,3072]{2,1,0:T(2,128)(2,1)} %reshape.227), calls=%async_computation.2 | async-start | bytes 1572864 | tf_op jit(solution)/shard_map/all_to_all | solution.py:124
  270.3 7.3 %copy-start.6 = (bf16[256,256]{1,0:T(8,128)(2,1)S(1)}, bf16[256,256]{1,0:T(8,128)(2,1)}, u32[]{:S(2)}) copy-start(bf16[256,256]{1,0:T(8,128)(2,1)} %param.20) | copy-start | bytes 393220
  270.4 7.3 %copy-start.8 = (bf16[256,256]{1,0:T(8,128)(2,1)S(1)}, bf16[256,256]{1,0:T(8,128)(2,1)}, u32[]{:S(2)}) copy-start(bf16[256,256]{1,0:T(8,128)(2,1)} %param.21) | copy-start | bytes 393220
  271.6 9.8 %copy-start.12 = (bf16[3,256]{1,0:T(4,128)(2,1)S(1)}, bf16[3,256]{1,0:T(4,128)(2,1)}, u32[]{:S(2)}) copy-start(bf16[3,256]{1,0:T(4,128)(2,1)} %param.22) | copy-start | bytes 4612
  272.7 21.2 %copy-start.4 = (bf16[256,512]{1,0:T(8,128)(2,1)}, bf16[256,512]{1,0:T(8,128)(2,1)S(1)}, u32[]{:S(2)}) copy-start(bf16[256,512]{1,0:T(8,128)(2,1)S(1)} %add_convert_fusion.1) | copy-start | bytes 786436
  272.7 19.2 %copy-start.3 = (bf16[2048,256]{1,0:T(8,128)(2,1)S(1)}, bf16[2048,256]{1,0:T(8,128)(2,1)}, u32[]{:S(2)}) copy-start(bf16[2048,256]{1,0:T(8,128)(2,1)} %param.23) | copy-start | bytes 3145732
  273.9 18.0 %all-to-all-start.3 = ((bf16[4,256,512]{1,2,0:T(8,128)(2,1)}), bf16[4,256,512]{1,2,0:T(8,128)(2,1)S(1)}, u32[]{:S(2)}, u32[]{:S(2)}) async-start(bf16[4,256,512]{1,2,0:T(8,128)(2,1)} %broadcast_in_dim.39), calls=%async_computation.3 | async-start | bytes 2097152 | tf_op jit(solution)/shard_map/all_to_all | solution.py:42
  277.7 4.4 %collective-permute-start = (f32[2,256]{1,0:T(2,128)S(1)}, f32[2,256]{1,0:T(2,128)S(1)}, u32[]{:S(2)}, u32[]{:S(2)}) collective-permute-start(f32[2,256]{1,0:T(2,128)S(1)} %slice.57), channel_id=1, source_target_pairs={{0,4},{4,8},{8,12},{12,16},{16,20},{20,24},{24,28},{28,32},{32,36}... | collective-permute-start | bytes 6152 | tf_op jit(solution)/shard_map/ppermute | solution.py:52
  296.2 34.8 %all-to-all-start.4 = ((bf16[64,32,256]{2,1,0:T(8,128)(2,1)}), bf16[64,32,256]{2,1,0:T(8,128)(2,1)S(1)}, u32[]{:S(2)}, u32[]{:S(2)}) async-start(bf16[64,32,256]{2,1,0:T(8,128)(2,1)} %bitcast.18), calls=%async_computation.4 | async-start | bytes 2097152 | tf_op jit(solution)/shard_map/all_to_all | solution.py:30
  302.9 4.0 %copy-start.17 = (f32[768,256]{1,0:T(8,128)S(1)}, f32[768,256]{1,0:T(8,128)}, u32[]{:S(2)}) copy-start(f32[768,256]{1,0:T(8,128)} %copy-done.16) | copy-start | bytes 2359300
  302.9 4.0 %copy-start.19 = (f32[768,256]{1,0:T(8,128)S(1)}, f32[768,256]{1,0:T(8,128)}, u32[]{:S(2)}) copy-start(f32[768,256]{1,0:T(8,128)} %copy-done.18) | copy-start | bytes 2359300
  306.9 6.5 %copy-start.11 = (bf16[768,256]{1,0:T(8,128)(2,1)S(1)}, bf16[768,256]{1,0:T(8,128)(2,1)}, u32[]{:S(2)}) copy-start(bf16[768,256]{1,0:T(8,128)(2,1)} %copy-done.10) | copy-start | bytes 1179652
  310.9 6.5 %copy-start.7 = (bf16[256,256]{1,0:T(8,128)(2,1)S(1)}, bf16[256,256]{1,0:T(8,128)(2,1)}, u32[]{:S(2)}) copy-start(bf16[256,256]{1,0:T(8,128)(2,1)} %param.20) | copy-start | bytes 393220
  310.9 7.3 %copy-start.9 = (bf16[256,256]{1,0:T(8,128)(2,1)S(1)}, bf16[256,256]{1,0:T(8,128)(2,1)}, u32[]{:S(2)}) copy-start(bf16[256,256]{1,0:T(8,128)(2,1)} %param.21) | copy-start | bytes 393220
  310.9 6.5 %collective-permute-start.1 = (f32[2,256]{1,0:T(2,128)S(1)}, f32[2,256]{1,0:T(2,128)S(1)}, u32[]{:S(2)}, u32[]{:S(2)}) collective-permute-start(f32[2,256]{1,0:T(2,128)S(1)} %slice.62), channel_id=1, source_target_pairs={{4,0},{8,4},{12,8},{16,12},{20,16},{24,20},{28,24},{32,28},{36,32}... | collective-permute-start | bytes 6152 | tf_op jit(solution)/shard_map/ppermute | solution.py:52
  313.4 18.4 %copy-start.1 = (bf16[1,2048,256]{2,1,0:T(8,128)(2,1)S(1)}, bf16[1,2048,256]{2,1,0:T(8,128)(2,1)}, u32[]{:S(2)}) copy-start(bf16[1,2048,256]{2,1,0:T(8,128)(2,1)} %param.16) | copy-start | bytes 3145732
Sparse Core Ops, SparseCore 0:
  99.5 65.8 all-gather.1
where the time goes:
time: 340 us; the launch traced here: 339 us
  waiting for transfers between devices  112 us (33%)
  blocking collectives  102 us (30%)
  local copies, waits for them, and re-layouts  40.7 us (12%)
  starting transfers between devices  28.6 us (8%)
  matrix products  25.4 us (7%)
  other arithmetic  15.7 us (5%)
  between operations  14.6 us (4%)
    all_gather x1, waiting for transfers between devices, sent_together(): lax.all_gather(both, axis, axis=dim, tiled=True)  66 us
    all_to_all x1, blocking collectives, in_one_piece(): lax.all_to_all(both, axis, split_axis=split_dim, concat_axis=concat_dim,...  62.5 us
    all_to_all x1, blocking collectives, summed_on_arrival(): lax.all_to_all(blocks, axis, split_axis=0, concat_axis=0, tiled=True)  39.7 us
    all_to_all x1, waiting for transfers between devices, per_device(): lax.all_to_all(shared_rows, 'sp', split_axis=1, concat_axis=0, tiled=True)  23 us
    all_to_all x1, waiting for transfers between devices, summed_on_arrival(): lax.all_to_all(blocks, axis, split_axis=0, concat_axis=0, tiled=True)  12.2 us
    all_to_all x1, starting transfers between devices, per_device(): lax.all_to_all(shared_rows, 'sp', split_axis=1, concat_axis=0, tiled=True)  12 us
    all_to_all x1, waiting for transfers between devices, copy_for_each(): return lax.all_to_all(copies, axis, split_axis=0, concat_axis=0, tiled=True)  9.72 us
  transfers between devices with their start and end apart: 6, of which 5 were waited for; matrix products, arithmetic and copies ran while one was open for 4% of the time, Pallas kernels for 0%

commit v1 on v0

--- a/solution.py
+++ b/solution.py
@@ -121,7 +121,14 @@
     )
     partial_low = partial_grad.astype(jnp.bfloat16)
     shared_rows = summed_on_arrival(partial_low, "tp", 2).astype(jnp.bfloat16)
-    back = lax.all_to_all(shared_rows, "sp", split_axis=1, concat_axis=0, tiled=True)
+
+    def _direct_routes_all(local_values):
+        a_next = lax.all_to_all(
+            jnp.stack(jnp.split(local_values, lax.axis_size("sp"), axis=1)), "sp", 0, 0
+        )
+        return jnp.concatenate(a_next, axis=0)
+
+    back = _direct_routes_all(shared_rows)
     back_flat = back.reshape(experts * capacity, feature_share)
     per_token = back_flat[target].astype(jnp.float32).reshape(tok_rows, top_k, feature_share)
     own_cot = lax.dynamic_slice_in_dim(cotangent, share_offset, feature_share, 1).astype(

time: 340 us -> 379 us (1.11)
  local copies, waits for them, and re-layouts: 40.7 us -> 78.2 us
  other arithmetic: 15.7 us -> 11.6 us
  waiting for transfers between devices: 112 us -> 116 us
    unnamed x46 -> x103, local copies, waits for them, and re-layouts: 5.82 us -> 41.6 us
    unnamed x1 -> x0, other arithmetic: 5.43 us -> none
    all_to_all x1, waiting for transfers between devices: 23 us -> 28.1 us  [_direct_routes_all(): lax.all_to_all(jnp.stack(jnp.split(local_values, lax.axis_size('sp'), axi...]
where the time goes in v1:
time: 379 us; the launch traced here: 378 us
  waiting for transfers between devices  116 us (31%)
  blocking collectives  102 us (27%)
  local copies, waits for them, and re-layouts  78.2 us (21%)
  starting transfers between devices  29.5 us (8%)
  matrix products  25.7 us (7%)
  between operations  14.5 us (4%)
  other arithmetic  11.6 us (3%)
    all_gather x1, waiting for transfers between devices, sent_together(): lax.all_gather(both, axis, axis=dim, tiled=True)  66 us
    all_to_all x1, blocking collectives, in_one_piece(): lax.all_to_all(both, axis, split_axis=split_dim, concat_axis=concat_dim,...  62.5 us
    unnamed x103, local copies, waits for them, and re-layouts  41.6 us
    all_to_all x1, blocking collectives, summed_on_arrival(): lax.all_to_all(blocks, axis, split_axis=0, concat_axis=0, tiled=True)  40 us
    all_to_all x1, waiting for transfers between devices, _direct_routes_all(): lax.all_to_all(jnp.stack(jnp.split(local_values, lax.axis_size('sp'), axi...  28.1 us
    all_to_all x1, waiting for transfers between devices, summed_on_arrival(): lax.all_to_all(blocks, axis, split_axis=0, concat_axis=0, tiled=True)  12.2 us
    all_to_all x1, starting transfers between devices, _direct_routes_all(): lax.all_to_all(jnp.stack(jnp.split(local_values, lax.axis_size('sp'), axi...  11.9 us
    all_to_all x1, waiting for transfers between devices, copy_for_each(): return lax.all_to_all(copies, axis, split_axis=0, concat_axis=0, tiled=True)  9.07 us
  transfers between devices with their start and end apart: 6, of which 5 were waited for; matrix products, arithmetic and copies ran while one was open for 4% of the time, Pallas kernels for 0%

profile of v1, /device:TPU:1, one launch (start us, length us, event | category | flops | bytes accessed | tf_op | source)
XLA Modules:
  0.0 378.0 jit_solution(11988881768943939928)
XLA Ops:
  7.2 0.8 broadcast_multiply_fusion
  8.0 0.8 copy.153
  9.4 1.2 reduce-window.6
  11.0 2.4 scatter_custom_fusion
  13.5 1.0 constant_dynamic-slice_fusion
  14.5 3.3 gather_fusion.2
  17.8 1.2 reshape.171
  19.4 5.0 %gather_fusion.1 = f32[768]{0:T(1024)S(1)} fusion(f32[512]{0:T(512)S(1)} %reshape.162, s32[1024]{0:T(1024)S(1)} %get-tuple-element.24), kind=kCustom, calls=%fused_computation.1 | custom fusion | bytes 9216 | tf_op jit(solution)/shard_map/gather | solution.py:92
  24.5 1.0 constant_dynamic-slice_fusion.1
  25.5 3.3 gather_fusion
  28.8 2.1 gather.15
  31.2 1.0 copy-done.1
  32.8 62.5 %all_to_all.32 = bf16[64,12,1024]{2,1,0:T(8,128)(2,1)S(1)} all-to-all(bf16[64,12,1024]{2,1,0:T(8,128)(2,1)S(1)} %pad_maximum_fusion), channel_id=1, replica_groups=mesh['sp'=64,'tp'=4] {'sp'}, dimensions={0} | all-to-all | bytes 3145728 | tf_op jit(solution)/shard_map/all_to_all | solution.py:10
  95.2 1.3 all_to_all.22
  96.6 1.5 fusion.41
  98.1 1.3 pad_maximum_fusion.1
  99.4 66.0 %all-gather.2.cloned.1.call-done = bf16[2,768,2048]{2,1,0:T(8,128)(2,1)} async-done(((bf16[2,768,512]{2,1,0:T(8,128)(2,1)}), bf16[2,768,2048]{2,1,0:T(8,128)(2,1)}) %all-gather.2.cloned.1.call-update) | async-done | bytes 6291472 | tf_op jit(solution)/shard_map/all_gather | solution.py:20
  165.4 3.0 fusion.6
  168.4 0.7 copy-done.13
  169.1 1.0 fusion.7
  170.6 1.2 multiply_convert_fusion.2
  171.8 1.0 fusion.8
  172.9 2.8 add_convert_fusion
  175.6 6.2 %reshape.168 = bf16[1,768,4,512]{3,2,1,0:T(4,128)(2,1)} reshape(bf16[768,2048]{1,0:T(8,128)(2,1)} %add_convert_fusion) | data formatting | bytes 6291456 | tf_op jit(solution)/shard_map/reshape | solution.py:25
  181.8 2.5 copy.162
  184.3 40.0 %all_to_all.33 = bf16[4,1,768,512]{3,2,1,0:T(8,128)(2,1)} all-to-all(bf16[4,1,768,512]{3,2,1,0:T(8,128)(2,1)S(1)} %bitcast.332), channel_id=1, replica_groups=mesh['sp'=64,'tp'=4] {'tp'}, dimensions={0} | all-to-all | bytes 6291456 | tf_op jit(solution)/shard_map/all_to_all | solution.py:30
  224.3 2.8 reduce_sum.45
  227.7 0.6 constant_dynamic-update-slice_fusion.62
  228.9 0.6 constant_dynamic-update-slice_fusion.60
  230.2 0.6 constant_dynamic-update-slice_fusion.58
  231.4 0.6 constant_dynamic-update-slice_fusion.56
  232.6 0.6 constant_dynamic-update-slice_fusion.54
  233.8 0.6 constant_dynamic-update-slice_fusion.52
  235.0 0.6 constant_dynamic-update-slice_fusion.50
  236.3 0.6 constant_dynamic-update-slice_fusion.48
  237.5 0.6 constant_dynamic-update-slice_fusion.46
  241.1 0.6 constant_dynamic-update-slice_fusion.40
  244.8 0.6 constant_dynamic-update-slice_fusion.34
  248.5 0.6 constant_dynamic-update-slice_fusion.28
  257.0 0.6 constant_dynamic-update-slice_fusion.14
  260.6 0.6 constant_dynamic-update-slice_fusion.8
  264.3 0.6 constant_dynamic-update-slice_fusion.2
  266.1 11.9 %all-to-all-start.2 = ((bf16[64,1,12,512]{3,2,1,0:T(8,128)(2,1)}), bf16[64,1,12,512]{3,2,1,0:T(8,128)(2,1)S(1)}, u32[]{:S(2)}, u32[]{:S(2)}) async-start(bf16[64,1,12,512]{3,2,1,0:T(8,128)(2,1)} %constant_dynamic-update-slice_fusion), calls=%async_computation.2 | async-start | bytes 2097152 | tf_op jit(solution)/shard_map/all_to_all | solution.py:126
  278.1 28.1 %all-to-all-done.2 = bf16[64,1,12,512]{3,2,1,0:T(8,128)(2,1)S(1)} async-done(((bf16[64,1,12,512]{3,2,1,0:T(8,128)(2,1)}), bf16[64,1,12,512]{3,2,1,0:T(8,128)(2,1)S(1)}, u32[]{:S(2)}, u32[]{:S(2)}) %all-to-all-start.2) | async-done | bytes 786464 | tf_op jit(solution)/shard_map/all_to_all | solution.py:126
  306.4 2.0 gather_fusion.3
  308.4 0.7 reshape.172
  309.0 1.2 reduce_sum.47
  310.3 1.0 add_convert_fusion.1
  311.5 1.0 broadcast_in_dim.39
  312.5 3.5 all-to-all-start.3
  316.1 4.1 %collective-permute-start = (f32[2,256]{1,0:T(2,128)S(1)}, f32[2,256]{1,0:T(2,128)S(1)}, u32[]{:S(2)}, u32[]{:S(2)}) collective-permute-start(f32[2,256]{1,0:T(2,128)S(1)} %slice.57), channel_id=1, source_target_pairs={{0,4},{4,8},{8,12},{12,16},{16,20},{20,24},{24,28},{28,32},{32,36}... | collective-permute-start | bytes 6152 | tf_op jit(solution)/shard_map/ppermute | solution.py:52
  320.3 0.7 collective-permute-done
  321.0 9.1 %all-to-all-done.3 = bf16[4,256,512]{1,2,0:T(8,128)(2,1)S(1)} async-done(((bf16[4,256,512]{1,2,0:T(8,128)(2,1)}), bf16[4,256,512]{1,2,0:T(8,128)(2,1)S(1)}, u32[]{:S(2)}, u32[]{:S(2)}) %all-to-all-start.3) | async-done | bytes 1048608 | tf_op jit(solution)/shard_map/all_to_all | solution.py:42
  330.1 2.4 multiply_convert_fusion.5
  332.4 2.3 convolution_convert_fusion
  334.8 7.4 %all-to-all-start.4 = ((bf16[64,32,256]{2,1,0:T(8,128)(2,1)}), bf16[64,32,256]{2,1,0:T(8,128)(2,1)S(1)}, u32[]{:S(2)}, u32[]{:S(2)}) async-start(bf16[64,32,256]{2,1,0:T(8,128)(2,1)} %bitcast.82), calls=%async_computation.4 | async-start | bytes 2097152 | tf_op jit(solution)/shard_map/all_to_all | solution.py:30
  342.2 4.0 %fusion.3 = bf16[1,2048,256]{2,1,0:T(8,128)(2,1)} fusion(bf16[768,256]{1,0:T(8,128)(2,1)S(1)} %get-tuple-element.15, bf16[2,768,2048]{2,1,0:T(8,128)(2,1)} %all-gather.2.cloned.1.call-done), kind=kOutput, calls=%fused_computation.15 | convolution fusion | flops 805830656 | bytes 4587520 | tf_op jit(solution)/shard_map/erd,erf->edf/dot_general | solution.py:112
  346.2 4.0 %fusion.5 = bf16[1,256,2048]{2,1,0:T(8,128)(2,1)} fusion(bf16[2,768,2048]{2,1,0:T(8,128)(2,1)} %all-gather.2.cloned.1.call-done, f32[768,256]{1,0:T(8,128)S(1)} %copy-done.18, f32[768,256]{1,0:T(8,128)S(1)} %copy-done.16), kind=kOutput, calls=%fused_computation.17 | convolution fusion | flops 807010304 | bytes 5767168 | tf_op jit(solution)/shard_map/erf,erd->efd/dot_general | solution.py:109
  350.2 2.5 collective-permute-start.1
  352.7 3.9 %fusion.4 = bf16[1,2048,256]{2,1,0:T(8,128)(2,1)} fusion(bf16[768,256]{1,0:T(8,128)(2,1)S(1)} %copy-done.9, bf16[2,768,2048]{2,1,0:T(8,128)(2,1)} %all-gather.2.cloned.1.call-done), kind=kOutput, calls=%fused_computation.16 | convolution fusion | flops 805830656 | bytes 4587520 | tf_op jit(solution)/shard_map/erd,erf->edf/dot_general | solution.py:115
  356.7 0.8 fusion.24
  357.4 0.7 fusion.25
  358.1 12.2 %all-to-all-done.4 = bf16[64,32,256]{2,1,0:T(8,128)(2,1)S(1)} async-done(((bf16[64,32,256]{2,1,0:T(8,128)(2,1)}), bf16[64,32,256]{2,1,0:T(8,128)(2,1)S(1)}, u32[]{:S(2)}, u32[]{:S(2)}) %all-to-all-start.4) | async-done | bytes 1048608 | tf_op jit(solution)/shard_map/all_to_all | solution.py:30
  370.4 0.8 convert_reduce_fusion
  (116 shorter events, 33.0 us)
Async XLA Ops:
  7.2 158.2 %copy-start = (bf16[1,2048,256]{2,1,0:T(8,128)(2,1)S(1)}, bf16[1,2048,256]{2,1,0:T(8,128)(2,1)}, u32[]{:S(2)}) copy-start(bf16[1,2048,256]{2,1,0:T(8,128)(2,1)} %param.16) | copy-start | bytes 3145732
  7.2 158.2 %all-gather.2.cloned.1.call-start = ((), (), s32[]{:S(2)}) async-start(), calls=%async_computation.5 | async-start | bytes 7864320 | tf_op jit(solution)/shard_map/all_gather | solution.py:20
  14.5 4.6 %copy-start.11 = (f32[256,2]{0,1:T(2,128)S(1)}, f32[256,2]{0,1:T(2,128)}, u32[]{:S(2)}) copy-start(f32[256,2]{0,1:T(2,128)} %param.15) | copy-start | bytes 6148
  31.0 1.2 copy-start.1
  99.4 69.0 %copy-start.3 = (bf16[1,2048,256]{2,1,0:T(8,128)(2,1)S(1)}, bf16[1,2048,256]{2,1,0:T(8,128)(2,1)}, u32[]{:S(2)}) copy-start(bf16[1,2048,256]{2,1,0:T(8,128)(2,1)} %param.17) | copy-start | bytes 3145732
  165.4 3.7 copy-start.13
  169.1 1.0 copy-start.15
  169.1 1.5 copy-start.14
  170.6 1.2 copy-start.17
  171.8 1.0 copy-start.8
  266.1 40.1 %all-to-all-start.2 = ((bf16[64,1,12,512]{3,2,1,0:T(8,128)(2,1)}), bf16[64,1,12,512]{3,2,1,0:T(8,128)(2,1)S(1)}, u32[]{:S(2)}, u32[]{:S(2)}) async-start(bf16[64,1,12,512]{3,2,1,0:T(8,128)(2,1)} %constant_dynamic-update-slice_fusion), calls=%async_computation.2 | async-start | bytes 2097152 | tf_op jit(solution)/shard_map/all_to_all | solution.py:126
  309.0 7.0 %copy-start.4 = (bf16[256,256]{1,0:T(8,128)(2,1)S(1)}, bf16[256,256]{1,0:T(8,128)(2,1)}, u32[]{:S(2)}) copy-start(bf16[256,256]{1,0:T(8,128)(2,1)} %param.20) | copy-start | bytes 393220
  309.0 7.0 %copy-start.6 = (bf16[256,256]{1,0:T(8,128)(2,1)S(1)}, bf16[256,256]{1,0:T(8,128)(2,1)}, u32[]{:S(2)}) copy-start(bf16[256,256]{1,0:T(8,128)(2,1)} %param.21) | copy-start | bytes 393220
  310.3 10.0 %copy-start.10 = (bf16[3,256]{1,0:T(4,128)(2,1)S(1)}, bf16[3,256]{1,0:T(4,128)(2,1)}, u32[]{:S(2)}) copy-start(bf16[3,256]{1,0:T(4,128)(2,1)} %param.22) | copy-start | bytes 4612
  311.3 21.1 %copy-start.2 = (bf16[256,512]{1,0:T(8,128)(2,1)}, bf16[256,512]{1,0:T(8,128)(2,1)S(1)}, u32[]{:S(2)}) copy-start(bf16[256,512]{1,0:T(8,128)(2,1)S(1)} %add_convert_fusion.1) | copy-start | bytes 786436
  312.5 17.5 %all-to-all-start.3 = ((bf16[4,256,512]{1,2,0:T(8,128)(2,1)}), bf16[4,256,512]{1,2,0:T(8,128)(2,1)S(1)}, u32[]{:S(2)}, u32[]{:S(2)}) async-start(bf16[4,256,512]{1,2,0:T(8,128)(2,1)} %broadcast_in_dim.39), calls=%async_computation.3 | async-start | bytes 2097152 | tf_op jit(solution)/shard_map/all_to_all | solution.py:42
  316.1 4.9 %collective-permute-start = (f32[2,256]{1,0:T(2,128)S(1)}, f32[2,256]{1,0:T(2,128)S(1)}, u32[]{:S(2)}, u32[]{:S(2)}) collective-permute-start(f32[2,256]{1,0:T(2,128)S(1)} %slice.57), channel_id=1, source_target_pairs={{0,4},{4,8},{8,12},{12,16},{16,20},{20,24},{24,28},{28,32},{32,36}... | collective-permute-start | bytes 6152 | tf_op jit(solution)/shard_map/ppermute | solution.py:52
  321.0 9.1 %copy-start.12 = (f32[2,256]{1,0:T(2,128)}, f32[2,256]{1,0:T(2,128)S(1)}, u32[]{:S(2)}) copy-start(f32[2,256]{1,0:T(2,128)S(1)} %collective-permute-done) | copy-start | bytes 6148
  334.8 35.6 %all-to-all-start.4 = ((bf16[64,32,256]{2,1,0:T(8,128)(2,1)}), bf16[64,32,256]{2,1,0:T(8,128)(2,1)S(1)}, u32[]{:S(2)}, u32[]{:S(2)}) async-start(bf16[64,32,256]{2,1,0:T(8,128)(2,1)} %bitcast.82), calls=%async_computation.4 | async-start | bytes 2097152 | tf_op jit(solution)/shard_map/all_to_all | solution.py:30
  342.2 4.0 %copy-start.16 = (f32[768,256]{1,0:T(8,128)S(1)}, f32[768,256]{1,0:T(8,128)}, u32[]{:S(2)}) copy-start(f32[768,256]{1,0:T(8,128)} %copy-done.15) | copy-start | bytes 2359300
  342.2 4.0 %copy-start.18 = (f32[768,256]{1,0:T(8,128)S(1)}, f32[768,256]{1,0:T(8,128)}, u32[]{:S(2)}) copy-start(f32[768,256]{1,0:T(8,128)} %copy-done.17) | copy-start | bytes 2359300
  346.2 6.5 %copy-start.9 = (bf16[768,256]{1,0:T(8,128)(2,1)S(1)}, bf16[768,256]{1,0:T(8,128)(2,1)}, u32[]{:S(2)}) copy-start(bf16[768,256]{1,0:T(8,128)(2,1)} %copy-done.8) | copy-start | bytes 1179652
  350.2 6.4 %copy-start.5 = (bf16[256,256]{1,0:T(8,128)(2,1)S(1)}, bf16[256,256]{1,0:T(8,128)(2,1)}, u32[]{:S(2)}) copy-start(bf16[256,256]{1,0:T(8,128)(2,1)} %param.20) | copy-start | bytes 393220
  350.2 7.2 %copy-start.7 = (bf16[256,256]{1,0:T(8,128)(2,1)S(1)}, bf16[256,256]{1,0:T(8,128)(2,1)}, u32[]{:S(2)}) copy-start(bf16[256,256]{1,0:T(8,128)(2,1)} %param.21) | copy-start | bytes 393220
  350.2 6.4 %collective-permute-start.1 = (f32[2,256]{1,0:T(2,128)S(1)}, f32[2,256]{1,0:T(2,128)S(1)}, u32[]{:S(2)}, u32[]{:S(2)}) collective-permute-start(f32[2,256]{1,0:T(2,128)S(1)} %slice.62), channel_id=1, source_target_pairs={{4,0},{8,4},{12,8},{16,12},{20,16},{24,20},{28,24},{32,28},{36,32}... | collective-permute-start | bytes 6152 | tf_op jit(solution)/shard_map/ppermute | solution.py:52
Sparse Core Ops, SparseCore 0:
  99.5 65.8 all-gather.1
